TPU v7x, 32 devices: a whole 2x2x4 slice. The times are simulated.
32 devices in a mesh: sp: 4 (over y, x), tp: 8 (over z, core).
Axes of the slice: x: 2, y: 2, z: 4, core: 2. Of those that a mesh axis runs over, the one named last changes fastest.
Arguments:
- tokens: bfloat16 [8192, 2048], P('sp', 'tp'), may hold values from -6 to 6
- norm_gain: float32 [2048], replicated, may hold values from 0.1 to 1.9
- w_key: bfloat16 [2048, 1024], P(None, 'tp'), may hold values from -0.125 to 0.125
- w_decay: bfloat16 [2048, 1024], P(None, 'tp'), may hold values from -0.125 to 0.125
- w_value: bfloat16 [2048, 512], replicated, may hold values from -0.125 to 0.125
- decay_bias: float32 [1024], P('tp'), may hold values from 0 to 8.5
- gate_drift: float32 [8192], P('sp'), may hold values from -1 to 1
- queries: bfloat16 [1024], P('tp'), may hold values from -6 to 6
- out_gain: float32 [4, 512], P(None, 'sp'), may hold values from 0.1 to 1.9
Outputs:
- state_cache: bfloat16 [1024, 512], P('tp', 'sp')
- first_read: float32 [4, 512], P(None, 'sp')
All inputs are finite; a program needn't handle non-finite values.
Results may differ from a plain program's by a relative error of at most 0.009.
Values may be sent and summed in bfloat16 or wider, within the bound.
A program may use at most 128 MiB of HBM per device.

v0:
```python
import jax
import jax.numpy as jnp
from jax import lax
from jax.sharding import PartitionSpec as P

QUERY_KEY_HEADS = 4
KEY_CHANNELS = 256
VALUE_CHANNELS = 512
EPS = 1e-06
GATE_NORM = 16.0


def body(tokens, norm_gain, w_key, w_decay, w_value, decay_bias, gate_drift, queries, out_gain):
    gathered = lax.all_gather(tokens, "tp", axis=1, tiled=True)
    rows_f32 = gathered.astype(jnp.float32)
    inverse_rms = lax.rsqrt(jnp.mean(rows_f32 * rows_f32, axis=1, keepdims=True) + EPS)
    normed = (rows_f32 * inverse_rms * norm_gain[None, :]).astype(jnp.bfloat16)
    key_proj = jnp.dot(normed, w_key, preferred_element_type=jnp.float32).astype(jnp.bfloat16)
    gate_pre = jnp.dot(normed, w_decay, preferred_element_type=jnp.float32).astype(jnp.bfloat16)
    value_proj = jnp.dot(normed, w_value, preferred_element_type=jnp.float32).astype(jnp.bfloat16)
    log_decay = (
        jax.nn.log_sigmoid(gate_pre.astype(jnp.float32) + decay_bias[None, :] + gate_drift[:, None])
        / GATE_NORM
    )
    suffix = lax.cumsum(log_decay, axis=0, reverse=True)
    weighted = (key_proj.astype(jnp.float32) * jnp.exp(suffix - log_decay)).astype(jnp.bfloat16)
    partial_value = lax.dot_general(
        weighted, value_proj, (((0,), (0,)), ((), ())), preferred_element_type=jnp.float32
    )
    total_decay = suffix[0]
    channels = partial_value.shape[0]
    span_count = lax.axis_size("sp")
    spread = jnp.broadcast_to(total_decay[None, :, None], (1, channels, span_count))
    blocks, totals = (
        lax.all_to_all(partial_value[None], "sp", split_axis=2, concat_axis=0, tiled=True),
        lax.all_to_all(spread, "sp", split_axis=2, concat_axis=0, tiled=True),
    )
    later_sum = lax.cumsum(totals, axis=0, reverse=True) - totals
    matrix_state = jnp.sum(jnp.exp(later_sum) * blocks, axis=0)
    state_cache = matrix_state.astype(jnp.bfloat16)
    channel_ids = lax.axis_index("tp") * channels + jnp.arange(channels, dtype=jnp.int32)
    owners = (channel_ids // KEY_CHANNELS)[:, None] == jnp.arange(QUERY_KEY_HEADS, dtype=jnp.int32)[
        None, :
    ]
    query_of_head = jnp.where(
        owners, queries.astype(jnp.float32)[:, None] * KEY_CHANNELS ** (-0.5), 0.0
    )
    part_read = lax.dot_general(
        query_of_head, matrix_state, (((0,), (0,)), ((), ())), precision=lax.Precision.HIGHEST
    )
    summed_read = lax.psum(part_read, "tp")
    squares = lax.psum(jnp.sum(summed_read * summed_read, axis=1), "sp")
    first_read = summed_read * lax.rsqrt(squares / VALUE_CHANNELS + EPS)[:, None] * out_gain
    return (state_cache, first_read)


def solution(mesh):
    return jax.shard_map(
        body,
        mesh=mesh,
        in_specs=(
            P("sp", "tp"),
            P(),
            P(None, "tp"),
            P(None, "tp"),
            P(),
            P("tp"),
            P("sp"),
            P("tp"),
            P(None, "sp"),
        ),
        out_specs=(P("tp", "sp"), P(None, "sp")),
        check_vma=False,
    )
```

profile of v0, /device:TPU:0, one launch (start us, length us, event | category | flops | bytes accessed | tf_op | source)
XLA Modules:
  0.0 171.0 jit_solution(2722808447826279931)
XLA Ops:
  7.2 0.0 copy-start
  7.2 0.0 copy-start.5
  7.2 0.0 copy-start.3
  7.2 0.0 copy-start.6
  7.2 0.0 copy-start.4
  7.2 0.0 all-gather.2.cloned.1.call-start
  7.3 0.7 all-gather.2.cloned.1.call-update
  8.0 0.7 convert_multiply_fusion.2
  8.7 86.2 %all-gather.2.cloned.1.call-done = bf16[2048,2048]{1,0:T(8,128)(2,1)} async-done(((bf16[2048,256]{1,0:T(8,128)(2,1)}), bf16[2048,2048]{1,0:T(8,128)(2,1)}) %all-gather.2.cloned.1.call-update) | async-done | bytes 8388624 | tf_op jit(solution)/shard_map/all_gather | solution.py:14
  94.9 0.0 copy-start.1
  94.9 5.2 %fusion = f32[2048]{0:T(1024)S(1)} fusion(bf16[2048,2048]{1,0:T(8,128)(2,1)} %all-gather.2.cloned.1.call-done), kind=kLoop, calls=%fused_computation.2 | loop fusion | flops 12580864 | bytes 8396800 | tf_op jit(solution)/shard_map/reduce_sum | solution.py:16
  100.1 0.0 copy-done.5
  100.1 0.0 copy-done.3
  100.1 0.0 copy-done.6
  100.1 0.0 copy-done.4
  100.1 0.5 copy-done.1
  100.6 4.7 %fusion.12 = (f32[128,2048]{0,1:T(8,128)S(1)}, f32[2048,128]{1,0:T(8,128)}) fusion(f32[2048]{0:T(1024)S(1)} %copy-done.4, f32[128]{0:T(128)S(1)} %copy-done.6, bf16[2048,128]{1,0:T(8,128)(2,1)S(1)} %copy-done.3, bf16[2048,2048]{1,0:T(8,128)(2,1)S(1)} %copy-done.1, f32[2048]{0:T(1024)S(1)} %copy-done.5, f32[2048]{0:T(1024)S(1)} %add_rsqrt_fusion), kind=kOutput, calls=%fused_computation.19 | convolution fusion | flops 1093926912 | bytes 11035136 | tf_op jit(solution)/shard_map/dot_general | solution.py:19
  105.4 2.6 %fusion.21 = f32[128,16,128]{0,1,2:T(8,128)S(1)} fusion(f32[128,16,128]{0,2,1:T(8,128)S(1)} %bitcast.44), kind=kOutput, calls=%fused_computation.30 | output fusion | flops 33292288 | bytes 2097152 | tf_op jit(solution)/shard_map/reduce-window
  108.0 0.1 broadcast_add_fusion
  108.1 0.3 copy.17
  108.4 0.6 broadcast_in_dim.19
  109.0 3.6 %all-to-all-start = ((f32[1,128,4]{1,0,2:T(1,128)}), f32[1,128,4]{1,0,2:T(1,128)S(1)}, u32[]{:S(2)}, u32[]{:S(2)}) async-start(f32[1,128,4]{1,0,2:T(1,128)} %broadcast_in_dim.19), calls=%async_computation | async-start | bytes 4096 | tf_op jit(solution)/shard_map/all_to_all | solution.py:36
  112.6 7.6 %fusion.9 = bf16[2048,128]{1,0:T(8,128)(2,1)} fusion(bf16[2048,128]{1,0:T(8,128)(2,1)} %param.11, f32[2048,128]{1,0:T(8,128)S(1)} %bitcast.43, f32[2048,128]{1,0:T(8,128)} %get-tuple-element.5, bf16[2048,2048]{1,0:T(8,128)(2,1)} %all-gather.2.cloned.1.call-done, f32[2048]{0:T(1024)S(1)} %copy-done.5, f32[2048]{0:T(1024)S(1)} %add_rsqrt_fusion), kind=kOutput, calls=%fused_computation.16 | convolution fusion | flops 1093926912 | bytes 11550720 | tf_op jit(solution)/shard_map/dot_general | solution.py:18
  120.2 0.0 copy-done
  120.2 0.0 copy-start.2
  120.2 10.2 %fusion.10 = f32[128,512]{0,1:T(8,128)} fusion(bf16[2048,128]{1,0:T(8,128)(2,1)} %fusion.9, bf16[2048,512]{1,0:T(8,128)(2,1)S(1)} %copy-done, bf16[2048,2048]{1,0:T(8,128)(2,1)} %all-gather.2.cloned.1.call-done, f32[2048]{0:T(1024)S(1)} %copy-done.5, f32[2048]{0:T(1024)S(1)} %add_rsqrt_fusion), kind=kOutput, calls=%fused_computation.17 | convolution fusion | flops 4581228544 | bytes 11288576 | tf_op jit(solution)/shard_map/dot_general | solution.py:27
  130.4 0.0 all-to-all-done
  130.5 4.2 %all-to-all-start.1 = ((f32[1,128,512]{1,0,2:T(1,128)}), f32[1,128,512]{1,0,2:T(1,128)S(1)}, u32[]{:S(2)}, u32[]{:S(2)}) async-start(f32[1,128,512]{1,0,2:T(1,128)} %bitcast.18), calls=%async_computation.1 | async-start | bytes 524288 | tf_op jit(solution)/shard_map/all_to_all | solution.py:35
  134.7 5.3 %all-to-all-done.1 = f32[1,128,512]{1,0,2:T(1,128)S(1)} async-done(((f32[1,128,512]{1,0,2:T(1,128)}), f32[1,128,512]{1,0,2:T(1,128)S(1)}, u32[]{:S(2)}, u32[]{:S(2)}) %all-to-all-start.1) | async-done | bytes 262176 | tf_op jit(solution)/shard_map/all_to_all | solution.py:35
  140.0 0.3 fusion.23
  140.3 13.6 %psum.14 = f32[4,128]{1,0:T(4,128)S(1)} all-reduce(f32[4,128]{1,0:T(4,128)S(1)} %fusion.23), channel_id=1, replica_groups=mesh['sp'=4,'tp'=8] {'tp'}, use_global_device_ids=true, to_apply=%region_5.6 | all-reduce | flops 512 | bytes 4096 | tf_op jit(solution)/shard_map/psum | solution.py:51
  153.9 0.1 multiply_reduce_fusion.1
  154.1 8.7 %psum.15 = f32[4]{0:T(128)S(1)} all-reduce(f32[4]{0:T(128)S(1)} %multiply_reduce_fusion.1), channel_id=1, replica_groups=mesh['sp'=4,'tp'=8] {'sp'}, use_global_device_ids=true, to_apply=%region_7.8 | all-reduce | flops 4 | bytes 32 | tf_op jit(solution)/shard_map/psum | solution.py:52
  162.8 0.7 copy.19
  163.5 0.0 copy-done.2
  163.5 0.6 multiply_multiply_fusion
  (11 shorter events, 0.1 us)
Async XLA Ops:
  7.2 113.1 %copy-start = (bf16[2048,512]{1,0:T(8,128)(2,1)S(1)}, bf16[2048,512]{1,0:T(8,128)(2,1)}, u32[]{:S(2)}) copy-start(bf16[2048,512]{1,0:T(8,128)(2,1)} %param.13) | copy-start | bytes 6291460
  7.2 92.9 %copy-start.5 = (f32[2048]{0:T(1024)S(1)}, f32[2048]{0:T(1024)}, u32[]{:S(2)}) copy-start(f32[2048]{0:T(1024)} %param.10) | copy-start | bytes 24580
  7.2 92.9 %copy-start.3 = (bf16[2048,128]{1,0:T(8,128)(2,1)S(1)}, bf16[2048,128]{1,0:T(8,128)(2,1)}, u32[]{:S(2)}) copy-start(bf16[2048,128]{1,0:T(8,128)(2,1)} %param.12) | copy-start | bytes 1572868
  7.2 92.9 %copy-start.6 = (f32[128]{0:T(128)S(1)}, f32[128]{0:T(128)}, u32[]{:S(2)}) copy-start(f32[128]{0:T(128)} %param.14) | copy-start | bytes 1540
  7.2 92.9 %copy-start.4 = (f32[2048]{0:T(1024)S(1)}, f32[2048]{0:T(1024)}, u32[]{:S(2)}) copy-start(f32[2048]{0:T(1024)} %param.15) | copy-start | bytes 24580
  7.2 87.6 %all-gather.2.cloned.1.call-start = ((), (), s32[]{:S(2)}) async-start(), calls=%async_computation.2 | async-start | bytes 9437184 | tf_op jit(solution)/shard_map/all_gather | solution.py:14
  94.9 5.8 %copy-start.1 = (bf16[2048,2048]{1,0:T(8,128)(2,1)S(1)}, bf16[2048,2048]{1,0:T(8,128)(2,1)}, u32[]{:S(2)}) copy-start(bf16[2048,2048]{1,0:T(8,128)(2,1)} %all-gather.2.cloned.1.call-done) | copy-start | bytes 25165828
  109.0 21.5 %all-to-all-start = ((f32[1,128,4]{1,0,2:T(1,128)}), f32[1,128,4]{1,0,2:T(1,128)S(1)}, u32[]{:S(2)}, u32[]{:S(2)}) async-start(f32[1,128,4]{1,0,2:T(1,128)} %broadcast_in_dim.19), calls=%async_computation | async-start | bytes 4096 | tf_op jit(solution)/shard_map/all_to_all | solution.py:36
  120.2 43.3 %copy-start.2 = (f32[4,128]{1,0:T(4,128)S(1)}, f32[4,128]{1,0:T(4,128)}, u32[]{:S(2)}) copy-start(f32[4,128]{1,0:T(4,128)} %param.17) | copy-start | bytes 6148
  130.5 9.6 %all-to-all-start.1 = ((f32[1,128,512]{1,0,2:T(1,128)}), f32[1,128,512]{1,0,2:T(1,128)S(1)}, u32[]{:S(2)}, u32[]{:S(2)}) async-start(f32[1,128,512]{1,0,2:T(1,128)} %bitcast.18), calls=%async_computation.1 | async-start | bytes 524288 | tf_op jit(solution)/shard_map/all_to_all | solution.py:35
Sparse Core Ops, SparseCore 0:
  9.6 85.1 all-gather.1
where the time goes:
time: 171 us
  waiting for transfers between devices  92.2 us (54%)
  matrix products  22.8 us (13%)
  blocking collectives  22.4 us (13%)
  between operations  14.2 us (8%)
  other arithmetic  9.45 us (6%)
  starting transfers between devices  7.88 us (5%)
  local copies, waits for them, and re-layouts  2.17 us (1%)
    all_gather x1, waiting for transfers between devices, body(): gathered = lax.all_gather(tokens, 'tp', axis=1, tiled=True)  86.2 us
    psum x1, blocking collectives, body(): summed_read = lax.psum(part_read, 'tp')  13.6 us
    dot_general x1, matrix products, body(): lax.dot_general(weighted, value_proj, (((0,), (0,)), ((), ())), preferred...  10.2 us
    psum x1, blocking collectives, body(): squares = lax.psum(jnp.sum(summed_read * summed_read, axis=1), 'sp')  8.74 us
    dot_general x1, matrix products, body(): jnp.dot(normed, w_key, preferred_element_type=jnp.float32)  7.58 us
    all_to_all x1, waiting for transfers between devices, body(): lax.all_to_all(partial_value[None], 'sp', split_axis=2, concat_axis=0, ti...  5.33 us
    reduce_sum x1, other arithmetic, body(): jnp.mean(rows_f32 * rows_f32, axis=1, keepdims=True) + EPS  5.23 us
    dot_general x1, matrix products, body(): jnp.dot(normed, w_decay, preferred_element_type=jnp.float32)  4.74 us
  transfers between devices with their start and end apart: 3, of which 2 were waited for; matrix products, arithmetic and copies ran while one was open for 11% of the time, Pallas kernels for 0%

commit v1 on v0

--- a/solution.py
+++ b/solution.py
@@ -1,3 +1,4 @@
+import functools
 import jax
 import jax.numpy as jnp
 from jax import lax
@@ -10,8 +11,28 @@
 GATE_NORM = 16.0
 
 
+def write_the_table(block_here, axis_name):
+    num_devices = lax.axis_size(axis_name)
+    blocks_here = [block_here]
+    nth = 0
+    while nth < num_devices - 1:
+        blocks_here.append(
+            lax.ppermute(
+                blocks_here[-1],
+                axis_name,
+                [(tick, (tick + 1) % num_devices) for tick in range(num_devices)],
+            )
+        )
+        nth += 1
+    w_next = jnp.concatenate(blocks_here[::-1], axis=1)
+    return jnp.roll(w_next, (lax.axis_index(axis_name) + 1) * block_here.shape[1], axis=1)
+
+
+rest_chunk_here = functools.partial(write_the_table, axis_name="tp")
+
+
 def body(tokens, norm_gain, w_key, w_decay, w_value, decay_bias, gate_drift, queries, out_gain):
-    gathered = lax.all_gather(tokens, "tp", axis=1, tiled=True)
+    gathered = rest_chunk_here(tokens)
     rows_f32 = gathered.astype(jnp.float32)
     inverse_rms = lax.rsqrt(jnp.mean(rows_f32 * rows_f32, axis=1, keepdims=True) + EPS)
     normed = (rows_f32 * inverse_rms * norm_gain[None, :]).astype(jnp.bfloat16)

time: 171 us -> 201 us (1.18)
  waiting for transfers between devices: 92.2 us -> 118 us
  local copies, waits for them, and re-layouts: 2.17 us -> 21.2 us
  between operations: 14.2 us -> 0.99 us
  other arithmetic: 9.45 us -> 6.04 us
    ppermute x0 -> x7, waiting for transfers between devices: none -> 112 us  [write_the_table(): lax.ppermute(blocks_here[-1], axis_name, [(tick, (tick + 1) % num_devices...]
    all_gather x1 -> x0, waiting for transfers between devices: 86.2 us -> none  [body(): gathered = lax.all_gather(tokens, 'tp', axis=1, tiled=True)]
    unnamed x15 -> x52, local copies, waits for them, and re-layouts: 1.24 us -> 20.1 us
    reduce_sum x1, other arithmetic: 5.23 us -> 1.71 us  [body(): jnp.mean(rows_f32 * rows_f32, axis=1, keepdims=True) + EPS]
  transfers between devices with their start and end apart: 3 -> 9, of which waited for: 2 -> 8; matrix products, arithmetic and copies ran while one was open for 11% -> 9% of each run, Pallas kernels for 0% -> 0%
where the time goes in v1:
time: 201 us
  waiting for transfers between devices  118 us (59%)
  matrix products  23.2 us (12%)
  blocking collectives  22.4 us (11%)
  local copies, waits for them, and re-layouts  21.2 us (11%)
  starting transfers between devices  8.96 us (4%)
  other arithmetic  6.04 us (3%)
    ppermute x7, waiting for transfers between devices, write_the_table(): lax.ppermute(blocks_here[-1], axis_name, [(tick, (tick + 1) % num_devices...  112 us
    unnamed x52, local copies, waits for them, and re-layouts  20.1 us
    psum x1, blocking collectives, body(): summed_read = lax.psum(part_read, 'tp')  13.6 us
    dot_general x1, matrix products, body(): lax.dot_general(weighted, value_proj, (((0,), (0,)), ((), ())), preferred...  10.2 us
    psum x1, blocking collectives, body(): squares = lax.psum(jnp.sum(summed_read * summed_read, axis=1), 'sp')  8.74 us
    dot_general x1, matrix products, body(): jnp.dot(normed, w_key, preferred_element_type=jnp.float32)  7.58 us
    all_to_all x1, waiting for transfers between devices, body(): lax.all_to_all(partial_value[None], 'sp', split_axis=2, concat_axis=0, ti...  5.33 us
    dot_general x1, matrix products, body(): jnp.dot(normed, w_decay, preferred_element_type=jnp.float32)  5.15 us
  transfers between devices with their start and end apart: 9, of which 8 were waited for; matrix products, arithmetic and copies ran while one was open for 9% of the time, Pallas kernels for 0%

profile of v1, /device:TPU:0, one launch (start us, length us, event | category | flops | bytes accessed | tf_op | source)
XLA Modules:
  0.0 200.5 jit_solution(13018355482418046786)
XLA Ops:
  0.6 0.0 copy-start
  0.6 0.0 copy-start.2
  0.7 0.5 collective-permute-start
  1.2 16.7 %collective-permute-done = bf16[2048,256]{1,0:T(8,128)(2,1)S(1)} collective-permute-done((bf16[2048,256]{1,0:T(8,128)(2,1)}, bf16[2048,256]{1,0:T(8,128)(2,1)S(1)}, u32[]{:S(2)}, u32[]{:S(2)}) %collective-permute-start) | collective-permute-done | bytes 1048608 | tf_op jit(solution)/shard_map/ppermute | solution.py:20
  17.9 1.0 copy-done.3
  18.9 0.0 collective-permute-start.1
  18.9 16.0 %collective-permute-done.1 = bf16[2048,256]{1,0:T(8,128)(2,1)S(1)} collective-permute-done((bf16[2048,256]{1,0:T(8,128)(2,1)S(1)}, bf16[2048,256]{1,0:T(8,128)(2,1)S(1)}, u32[]{:S(2)}, u32[]{:S(2)}) %collective-permute-start.1) | collective-permute-done | bytes 1048608 | tf_op jit(solution)/shard_map/ppermute | solution.py:20
  34.9 1.0 copy-done.5
  36.0 0.0 collective-permute-start.2
  36.0 16.0 %collective-permute-done.2 = bf16[2048,256]{1,0:T(8,128)(2,1)S(1)} collective-permute-done((bf16[2048,256]{1,0:T(8,128)(2,1)S(1)}, bf16[2048,256]{1,0:T(8,128)(2,1)S(1)}, u32[]{:S(2)}, u32[]{:S(2)}) %collective-permute-start.2) | collective-permute-done | bytes 1048608 | tf_op jit(solution)/shard_map/ppermute | solution.py:20
  52.0 1.0 copy-done.7
  53.0 0.0 collective-permute-start.3
  53.0 16.0 %collective-permute-done.3 = bf16[2048,256]{1,0:T(8,128)(2,1)S(1)} collective-permute-done((bf16[2048,256]{1,0:T(8,128)(2,1)S(1)}, bf16[2048,256]{1,0:T(8,128)(2,1)S(1)}, u32[]{:S(2)}, u32[]{:S(2)}) %collective-permute-start.3) | collective-permute-done | bytes 1048608 | tf_op jit(solution)/shard_map/ppermute | solution.py:20
  69.0 1.0 copy-done.9
  70.0 0.0 collective-permute-start.4
  70.0 16.0 %collective-permute-done.4 = bf16[2048,256]{1,0:T(8,128)(2,1)S(1)} collective-permute-done((bf16[2048,256]{1,0:T(8,128)(2,1)S(1)}, bf16[2048,256]{1,0:T(8,128)(2,1)S(1)}, u32[]{:S(2)}, u32[]{:S(2)}) %collective-permute-start.4) | collective-permute-done | bytes 1048608 | tf_op jit(solution)/shard_map/ppermute | solution.py:20
  86.0 1.0 copy-done.11
  87.0 0.0 collective-permute-start.5
  87.0 16.1 %collective-permute-done.5 = bf16[2048,256]{1,0:T(8,128)(2,1)} collective-permute-done((bf16[2048,256]{1,0:T(8,128)(2,1)S(1)}, bf16[2048,256]{1,0:T(8,128)(2,1)}, u32[]{:S(2)}, u32[]{:S(2)}) %collective-permute-start.5) | collective-permute-done | bytes 1048608 | tf_op jit(solution)/shard_map/ppermute | solution.py:20
  103.1 0.0 collective-permute-start.6
  103.1 0.0 copy-start.6
  103.2 0.8 convert_multiply_fusion.2
  104.0 15.5 %collective-permute-done.6 = bf16[2048,256]{1,0:T(8,128)(2,1)} collective-permute-done((bf16[2048,256]{1,0:T(8,128)(2,1)}, bf16[2048,256]{1,0:T(8,128)(2,1)}, u32[]{:S(2)}, u32[]{:S(2)}) %collective-permute-start.6) | collective-permute-done | bytes 1048608 | tf_op jit(solution)/shard_map/ppermute | solution.py:20
  119.5 1.4 constant_dynamic-update-slice_fusion.15
  120.8 1.4 constant_dynamic-update-slice_fusion.14
  122.2 1.4 constant_dynamic-update-slice_fusion.13
  123.6 1.4 constant_dynamic-update-slice_fusion.12
  124.9 0.0 copy-start.14
  125.0 0.0 copy-start.15
  125.0 0.0 copy-start.16
  125.0 0.0 copy-start.17
  125.0 1.4 constant_dynamic-update-slice_fusion.11
  126.4 1.4 constant_dynamic-update-slice_fusion.10
  127.8 1.4 constant_dynamic-update-slice_fusion.9
  129.2 1.4 constant_dynamic-update-slice_fusion.8
  130.5 1.4 constant_dynamic-update-slice_fusion.7
  131.9 1.4 constant_dynamic-update-slice_fusion.6
  133.3 0.1 constant_dynamic-update-slice_fusion.5
  133.4 0.1 constant_dynamic-update-slice_fusion.4
  133.6 0.1 constant_dynamic-update-slice_fusion.3
  133.8 0.1 constant_dynamic-update-slice_fusion.2
  133.9 0.0 copy-done.4
  133.9 0.1 constant_dynamic-update-slice_fusion.1
  134.1 0.1 constant_dynamic-update-slice_fusion
  134.2 1.7 fusion
  136.0 5.1 %fusion.12 = (f32[128,2048]{0,1:T(8,128)S(1)}, f32[2048,128]{1,0:T(8,128)}) fusion(f32[2048]{0:T(1024)S(1)} %copy-done.15, f32[128]{0:T(128)S(1)} %copy-done.17, bf16[2048,128]{1,0:T(8,128)(2,1)S(1)} %copy-done.14, f32[2048]{0:T(1024)S(1)} %copy-done.16, f32[2048]{0:T(1024)S(1)} %add_rsqrt_fusion, ...), kind=kOutput, calls=%fused_computation.19 | convolution fusion | flops 1093926912 | bytes 11035140 | tf_op jit(solution)/shard_map/dot_general | solution.py:40
  141.1 2.6 %fusion.21 = f32[128,16,128]{0,1,2:T(8,128)S(1)} fusion(f32[128,16,128]{0,2,1:T(8,128)S(1)} %bitcast.44), kind=kOutput, calls=%fused_computation.30 | output fusion | flops 33292288 | bytes 2097152 | tf_op jit(solution)/shard_map/reduce-window
  143.7 0.1 broadcast_add_fusion
  143.8 0.3 copy.17
  144.2 0.6 broadcast_in_dim.19
  144.8 4.2 %all-to-all-start = ((f32[1,128,4]{1,0,2:T(1,128)}), f32[1,128,4]{1,0,2:T(1,128)S(1)}, u32[]{:S(2)}, u32[]{:S(2)}) async-start(f32[1,128,4]{1,0,2:T(1,128)} %broadcast_in_dim.19), calls=%async_computation | async-start | bytes 4096 | tf_op jit(solution)/shard_map/all_to_all | solution.py:57
  149.0 7.6 %fusion.9 = bf16[2048,128]{1,0:T(8,128)(2,1)} fusion(bf16[2048,128]{1,0:T(8,128)(2,1)} %param.11, f32[2048,128]{1,0:T(8,128)S(1)} %bitcast.43, f32[2048,128]{1,0:T(8,128)} %get-tuple-element.5, f32[2048]{0:T(1024)S(1)} %copy-done.16, f32[2048]{0:T(1024)S(1)} %add_rsqrt_fusion, bf16[2048,4096]{1,0:T(8,128)(2,1)} %copy-done.1, s32[]{:T(128)S(6)} %select_n.35), kind=kOutput, calls=%fused_computation.16 | convolution fusion | flops 1093926912 | bytes 11550724 | tf_op jit(solution)/shard_map/dot_general | solution.py:39
  156.6 0.0 copy-done
  156.6 10.2 %fusion.10 = f32[128,512]{0,1:T(8,128)} fusion(bf16[2048,128]{1,0:T(8,128)(2,1)} %fusion.9, bf16[2048,512]{1,0:T(8,128)(2,1)S(1)} %copy-done, f32[2048]{0:T(1024)S(1)} %copy-done.16, f32[2048]{0:T(1024)S(1)} %add_rsqrt_fusion, bf16[2048,4096]{1,0:T(8,128)(2,1)} %copy-done.1, s32[]{:T(128)S(6)} %select_n.35), kind=kOutput, calls=%fused_computation.17 | convolution fusion | flops 4581228544 | bytes 11288580 | tf_op jit(solution)/shard_map/dot_general | solution.py:48
  166.8 0.0 all-to-all-done
  166.8 4.2 %all-to-all-start.1 = ((f32[1,128,512]{1,0,2:T(1,128)}), f32[1,128,512]{1,0,2:T(1,128)S(1)}, u32[]{:S(2)}, u32[]{:S(2)}) async-start(f32[1,128,512]{1,0,2:T(1,128)} %bitcast.18), calls=%async_computation.1 | async-start | bytes 524288 | tf_op jit(solution)/shard_map/all_to_all | solution.py:56
  171.0 5.3 %all-to-all-done.1 = f32[1,128,512]{1,0,2:T(1,128)S(1)} async-done(((f32[1,128,512]{1,0,2:T(1,128)}), f32[1,128,512]{1,0,2:T(1,128)S(1)}, u32[]{:S(2)}, u32[]{:S(2)}) %all-to-all-start.1) | async-done | bytes 262176 | tf_op jit(solution)/shard_map/all_to_all | solution.py:56
  176.4 0.3 fusion.23
  176.7 13.6 %psum.14 = f32[4,128]{1,0:T(4,128)S(1)} all-reduce(f32[4,128]{1,0:T(4,128)S(1)} %fusion.23), channel_id=1, replica_groups=mesh['sp'=4,'tp'=8] {'tp'}, use_global_device_ids=true, to_apply=%region_5.6 | all-reduce | flops 512 | bytes 4096 | tf_op jit(solution)/shard_map/psum | solution.py:72
  190.3 0.1 multiply_reduce_fusion.1
  190.4 8.7 %psum.15 = f32[4]{0:T(128)S(1)} all-reduce(f32[4]{0:T(128)S(1)} %multiply_reduce_fusion.1), channel_id=1, replica_groups=mesh['sp'=4,'tp'=8] {'sp'}, use_global_device_ids=true, to_apply=%region_7.8 | all-reduce | flops 4 | bytes 32 | tf_op jit(solution)/shard_map/psum | solution.py:73
  199.1 0.7 copy.19
  199.9 0.0 copy-done.13
  199.9 0.6 multiply_multiply_fusion
  (32 shorter events, 0.2 us)
Async XLA Ops:
  0.6 155.9 %copy-start = (bf16[2048,512]{1,0:T(8,128)(2,1)S(1)}, bf16[2048,512]{1,0:T(8,128)(2,1)}, u32[]{:S(2)}) copy-start(bf16[2048,512]{1,0:T(8,128)(2,1)} %param.13) | copy-start | bytes 6291460
  0.6 133.4 %copy-start.2 = (bf16[2048,256]{1,0:T(8,128)(2,1)S(1)}, bf16[2048,256]{1,0:T(8,128)(2,1)}, u32[]{:S(2)}) copy-start(bf16[2048,256]{1,0:T(8,128)(2,1)} %param.9) | copy-start | bytes 3145732
  0.7 17.3 %collective-permute-start = (bf16[2048,256]{1,0:T(8,128)(2,1)}, bf16[2048,256]{1,0:T(8,128)(2,1)S(1)}, u32[]{:S(2)}, u32[]{:S(2)}) collective-permute-start(bf16[2048,256]{1,0:T(8,128)(2,1)} %param.9), channel_id=1, source_target_pairs={{0,1},{1,2},{2,3},{3,4},{4,5},{5,6},{6,7},{7,0},{8,9},{9,10},{10,1... | collective-permute-start | bytes 3145736 | tf_op jit(solution)/shard_map/ppermute | solution.py:20
  17.9 1.0 copy-start.3
  18.9 16.0 %collective-permute-start.1 = (bf16[2048,256]{1,0:T(8,128)(2,1)S(1)}, bf16[2048,256]{1,0:T(8,128)(2,1)S(1)}, u32[]{:S(2)}, u32[]{:S(2)}) collective-permute-start(bf16[2048,256]{1,0:T(8,128)(2,1)S(1)} %collective-permute-done), channel_id=1, source_target_pairs={{0,1},{1,2},{2,3},{3,4},{4,5},{5,6},{6,7},{7,0},{8,9},{9,10},{10,1... | collective-permute-start | bytes 3145736 | tf_op jit(solution)/shard_map/ppermute | solution.py:20
  34.9 1.0 copy-start.5
  36.0 16.0 %collective-permute-start.2 = (bf16[2048,256]{1,0:T(8,128)(2,1)S(1)}, bf16[2048,256]{1,0:T(8,128)(2,1)S(1)}, u32[]{:S(2)}, u32[]{:S(2)}) collective-permute-start(bf16[2048,256]{1,0:T(8,128)(2,1)S(1)} %collective-permute-done.1), channel_id=1, source_target_pairs={{0,1},{1,2},{2,3},{3,4},{4,5},{5,6},{6,7},{7,0},{8,9},{9,10},{10,1... | collective-permute-start | bytes 3145736 | tf_op jit(solution)/shard_map/ppermute | solution.py:20
  52.0 1.0 copy-start.7
  53.0 16.0 %collective-permute-start.3 = (bf16[2048,256]{1,0:T(8,128)(2,1)S(1)}, bf16[2048,256]{1,0:T(8,128)(2,1)S(1)}, u32[]{:S(2)}, u32[]{:S(2)}) collective-permute-start(bf16[2048,256]{1,0:T(8,128)(2,1)S(1)} %collective-permute-done.2), channel_id=1, source_target_pairs={{0,1},{1,2},{2,3},{3,4},{4,5},{5,6},{6,7},{7,0},{8,9},{9,10},{10,1... | collective-permute-start | bytes 3145736 | tf_op jit(solution)/shard_map/ppermute | solution.py:20
  69.0 1.0 copy-start.9
  70.0 16.0 %collective-permute-start.4 = (bf16[2048,256]{1,0:T(8,128)(2,1)S(1)}, bf16[2048,256]{1,0:T(8,128)(2,1)S(1)}, u32[]{:S(2)}, u32[]{:S(2)}) collective-permute-start(bf16[2048,256]{1,0:T(8,128)(2,1)S(1)} %collective-permute-done.3), channel_id=1, source_target_pairs={{0,1},{1,2},{2,3},{3,4},{4,5},{5,6},{6,7},{7,0},{8,9},{9,10},{10,1... | collective-permute-start | bytes 3145736 | tf_op jit(solution)/shard_map/ppermute | solution.py:20
  86.0 1.0 copy-start.11
  87.0 16.1 %collective-permute-start.5 = (bf16[2048,256]{1,0:T(8,128)(2,1)S(1)}, bf16[2048,256]{1,0:T(8,128)(2,1)}, u32[]{:S(2)}, u32[]{:S(2)}) collective-permute-start(bf16[2048,256]{1,0:T(8,128)(2,1)S(1)} %collective-permute-done.4), channel_id=1, source_target_pairs={{0,1},{1,2},{2,3},{3,4},{4,5},{5,6},{6,7},{7,0},{8,9},{9,10},{10,1... | collective-permute-start | bytes 3145736 | tf_op jit(solution)/shard_map/ppermute | solution.py:20
  103.1 16.3 %collective-permute-start.6 = (bf16[2048,256]{1,0:T(8,128)(2,1)}, bf16[2048,256]{1,0:T(8,128)(2,1)}, u32[]{:S(2)}, u32[]{:S(2)}) collective-permute-start(bf16[2048,256]{1,0:T(8,128)(2,1)} %collective-permute-done.5), channel_id=1, source_target_pairs={{0,1},{1,2},{2,3},{3,4},{4,5},{5,6},{6,7},{7,0},{8,9},{9,10},{10,1... | collective-permute-start | bytes 3145736 | tf_op jit(solution)/shard_map/ppermute | solution.py:20
  103.1 30.2 %copy-start.12 = (bf16[2048,256]{1,0:T(8,128)(2,1)S(1)}, bf16[2048,256]{1,0:T(8,128)(2,1)}, u32[]{:S(2)}) copy-start(bf16[2048,256]{1,0:T(8,128)(2,1)} %copy-done.11) | copy-start | bytes 3145732
  103.1 30.3 %copy-start.10 = (bf16[2048,256]{1,0:T(8,128)(2,1)S(1)}, bf16[2048,256]{1,0:T(8,128)(2,1)}, u32[]{:S(2)}) copy-start(bf16[2048,256]{1,0:T(8,128)(2,1)} %copy-done.9) | copy-start | bytes 3145732
  103.1 30.5 %copy-start.8 = (bf16[2048,256]{1,0:T(8,128)(2,1)S(1)}, bf16[2048,256]{1,0:T(8,128)(2,1)}, u32[]{:S(2)}) copy-start(bf16[2048,256]{1,0:T(8,128)(2,1)} %copy-done.7) | copy-start | bytes 3145732
  103.1 30.6 %copy-start.6 = (bf16[2048,256]{1,0:T(8,128)(2,1)S(1)}, bf16[2048,256]{1,0:T(8,128)(2,1)}, u32[]{:S(2)}) copy-start(bf16[2048,256]{1,0:T(8,128)(2,1)} %copy-done.5) | copy-start | bytes 3145732
  103.1 30.8 %copy-start.4 = (bf16[2048,256]{1,0:T(8,128)(2,1)S(1)}, bf16[2048,256]{1,0:T(8,128)(2,1)}, u32[]{:S(2)}) copy-start(bf16[2048,256]{1,0:T(8,128)(2,1)} %copy-done.3) | copy-start | bytes 3145732
  124.9 11.0 %copy-start.14 = (bf16[2048,128]{1,0:T(8,128)(2,1)S(1)}, bf16[2048,128]{1,0:T(8,128)(2,1)}, u32[]{:S(2)}) copy-start(bf16[2048,128]{1,0:T(8,128)(2,1)} %param.12) | copy-start | bytes 1572868
  125.0 11.0 %copy-start.15 = (f32[2048]{0:T(1024)S(1)}, f32[2048]{0:T(1024)}, u32[]{:S(2)}) copy-start(f32[2048]{0:T(1024)} %param.15) | copy-start | bytes 24580
  125.0 11.0 %copy-start.16 = (f32[2048]{0:T(1024)S(1)}, f32[2048]{0:T(1024)}, u32[]{:S(2)}) copy-start(f32[2048]{0:T(1024)} %param.10) | copy-start | bytes 24580
  125.0 11.0 %copy-start.17 = (f32[128]{0:T(128)S(1)}, f32[128]{0:T(128)}, u32[]{:S(2)}) copy-start(f32[128]{0:T(128)} %param.14) | copy-start | bytes 1540
  134.2 6.9 %copy-start.1 = (bf16[2048,4096]{1,0:T(8,128)(2,1)}, bf16[2048,4096]{1,0:T(8,128)(2,1)S(1)}, u32[]{:S(2)}) copy-start(bf16[2048,4096]{1,0:T(8,128)(2,1)S(1)} %constant_dynamic-update-slice_fusion) | copy-start | bytes 50331652
  144.8 22.0 %all-to-all-start = ((f32[1,128,4]{1,0,2:T(1,128)}), f32[1,128,4]{1,0,2:T(1,128)S(1)}, u32[]{:S(2)}, u32[]{:S(2)}) async-start(f32[1,128,4]{1,0,2:T(1,128)} %broadcast_in_dim.19), calls=%async_computation | async-start | bytes 4096 | tf_op jit(solution)/shard_map/all_to_all | solution.py:57
  156.6 43.3 %copy-start.13 = (f32[4,128]{1,0:T(4,128)S(1)}, f32[4,128]{1,0:T(4,128)}, u32[]{:S(2)}) copy-start(f32[4,128]{1,0:T(4,128)} %param.17) | copy-start | bytes 6148
  166.8 9.6 %all-to-all-start.1 = ((f32[1,128,512]{1,0,2:T(1,128)}), f32[1,128,512]{1,0,2:T(1,128)S(1)}, u32[]{:S(2)}, u32[]{:S(2)}) async-start(f32[1,128,512]{1,0,2:T(1,128)} %bitcast.18), calls=%async_computation.1 | async-start | bytes 524288 | tf_op jit(solution)/shard_map/all_to_all | solution.py:56
